TPU v7x, 256 devices: a whole 4x4x8 slice. The times are simulated.
256 devices in a mesh: ep: 64 (over z, y, core), tp: 4 (over x).
Axes of the slice: x: 4, y: 4, z: 8, core: 2. Of those that a mesh axis runs over, the one named last changes fastest.
Arguments:
- query_latent: bfloat16 [8192, 768], P('ep'), may hold values from -6 to 6
- keyval_latent: bfloat16 [8192, 512], P('ep'), may hold values from -6 to 6
- rotary_key: bfloat16 [8192, 32], P('ep'), may hold values from -6 to 6
- query_gain: float32 [768], replicated, may hold values from 0.3 to 48
- keyval_gain: float32 [512], replicated, may hold values from 0.1 to 1.9
- query_weight: bfloat16 [768, 1536], P(None, 'tp'), may hold values from -0.21875 to 0.21875
- keyval_weight: bfloat16 [512, 2048], P(None, 'tp'), may hold values from -0.25 to 0.25
- output_weight: bfloat16 [1024, 2048], P('tp'), may hold values from -0.1875 to 0.1875
- output_gain: float32 [2048], replicated, may hold values from 0.1 to 1.9
- second_rows: bfloat16 [8192, 2048], P('ep'), may hold values from -6 to 6
- second_gain: float32 [2048], replicated, may hold values from 0.1 to 1.9
- route_ids: int32 [8192, 4], P('ep'), may hold values from 0 to 63, all different within a row; in each aligned block of 128 rows (0 to 127, 128 to 255, ...) at most 16 rows name the same one
- route_weights: float32 [8192, 4], P('ep'), may hold values from 0.1 to 1
- gate_weight: bfloat16 [64, 2048, 1024], P('ep', None, 'tp'), may hold values from -0.125 to 0.125
- up_weight: bfloat16 [64, 2048, 1024], P('ep', None, 'tp'), may hold values from -0.125 to 0.125
- down_weight: bfloat16 [64, 1024, 2048], P('ep', 'tp'), may hold values from -0.1875 to 0.1875
- shared_gate: bfloat16 [2048, 512], P(None, 'tp'), may hold values from -0.125 to 0.125
- shared_up: bfloat16 [2048, 512], P(None, 'tp'), may hold values from -0.125 to 0.125
- shared_down: bfloat16 [512, 2048], P('tp'), may hold values from -0.25 to 0.25
Outputs:
- mixed: bfloat16 [8192, 2048], P(('ep', 'tp'))
- expert_mix: bfloat16 [8192, 2048], P('ep', 'tp')
Inputs may be any that keep to these rules, and one draw needn't show every extreme that they name: `route_ids`: each row names 4 different experts. Among the rows of one index of ep (aligned blocks of 128 rows) no expert is named more than 16 times, a bound that some expert reaches in some blocks.
All inputs are finite; a program needn't handle non-finite values.
Results may differ from a plain program's by a relative error of at most 0.023.
The roundings to bfloat16 on the way count: a program that leaves them out, or rounds other values in their place, can miss the bound.
Values may be sent and summed in bfloat16 or wider, within the bound.
A program may use at most 128 MiB of HBM per device.

v0:
```python
import jax
import jax.numpy as jnp
from jax import lax
from jax.sharding import PartitionSpec as P

NOPE = 64
ROPE = 32
VDIM = 64


EPS = 1e-06
ROPE_BASE = 10000.0


def side_by_side(arrays, axis, dim, along):
    both = jnp.concatenate(arrays, axis=along)
    result, at, gathered = (lax.all_gather(both, axis, axis=dim, tiled=True), 0, [])
    for a in arrays:
        gathered.append(lax.slice_in_dim(result, at, at + a.shape[along], axis=along))
        at += a.shape[along]
    return tuple(gathered)


def cut_along(shard, dim, size):
    lengths = shard.shape
    pieces = shard.reshape(*lengths[:dim], size, lengths[dim] // size, *lengths[dim + 1 :])
    return jnp.moveaxis(pieces, dim, 0)


def sent_and_summed(shard, axis, dim):
    pieces = cut_along(shard, dim, lax.axis_size(axis))
    arrived = lax.all_to_all(pieces, axis, split_axis=0, concat_axis=0, tiled=True)
    return arrived.astype(jnp.float32).sum(axis=0)


def rms_scale(values, gain_vec):
    widened = values.astype(jnp.float32)
    normed = widened * lax.rsqrt(jnp.mean(widened * widened, -1, keepdims=True) + EPS)
    return (normed * gain_vec).astype(jnp.bfloat16)


def rotate(values, positions):
    half_width = values.shape[-1] // 2
    inverse = 1.0 / ROPE_BASE ** (
        jnp.arange(half_width, dtype=jnp.float32) * 2.0 / (2 * half_width)
    )
    angles = positions[:, None] * inverse[None, :]
    cosine = jnp.cos(angles)
    sine_vals = jnp.sin(angles)
    if values.ndim == 3:
        cosine = cosine[:, None, :]
        sine_vals = sine_vals[:, None, :]
    first_half = values[..., :half_width]
    second = values[..., half_width:]
    return jnp.concatenate(
        [first_half * cosine - second * sine_vals, first_half * sine_vals + second * cosine], -1
    )


def per_device(
    query_latent,
    keyval_latent,
    rotary_key,
    query_gain,
    keyval_gain,
    query_weight,
    keyval_weight,
    output_weight,
    output_gain,
    second_rows,
    second_gain,
    route_ids,
    route_weights,
    gate_weight,
    up_weight,
    down_weight,
    shared_gate,
    shared_up,
    shared_down,
):
    first_rows = query_latent.shape[0]
    tp_count = lax.axis_size("tp")
    ep_count = lax.axis_size("ep")
    head_count = query_weight.shape[1] // (NOPE + ROPE)
    positions = (lax.axis_index("ep") * first_rows).astype(jnp.float32) + jnp.arange(
        first_rows, dtype=jnp.float32
    )
    queries = jnp.dot(
        rms_scale(query_latent, query_gain), query_weight, preferred_element_type=jnp.float32
    ).reshape(first_rows, head_count, NOPE + ROPE)
    queries = jnp.concatenate(
        [queries[..., :NOPE], rotate(queries[..., NOPE:], positions)], -1
    ).astype(jnp.bfloat16)
    query_plain = queries[..., :NOPE]
    query_turned = queries[..., NOPE:]
    kv_normed = rms_scale(keyval_latent, keyval_gain)
    key_rot = rotate(rotary_key.astype(jnp.float32), positions).astype(jnp.bfloat16)
    score_scale = (NOPE + ROPE) ** (-0.5)
    keyvals = jnp.dot(kv_normed, keyval_weight, preferred_element_type=jnp.float32).astype(
        jnp.bfloat16
    )
    highest = jnp.full((head_count, first_rows), -jnp.inf, jnp.float32)
    denominator = jnp.zeros((head_count, first_rows), jnp.float32)
    accumulated = jnp.zeros((first_rows, head_count, VDIM), jnp.float32)
    keyval_piece, rot_piece = side_by_side((keyvals, key_rot), "ep", 0, 1)
    key_count = keyval_piece.shape[0]
    keyval_heads = keyval_piece.reshape(key_count, head_count, NOPE + VDIM)
    scores = jnp.einsum(
        "qhd,khd->hqk", query_plain, keyval_heads[..., :NOPE], preferred_element_type=jnp.float32
    )
    scores = (
        scores
        + jnp.einsum("qhr,kr->hqk", query_turned, rot_piece, preferred_element_type=jnp.float32)
    ) * score_scale
    new_high = jnp.max(scores, -1)
    exponent = jnp.exp(scores - new_high[..., None])
    rescale = jnp.exp(highest - new_high)
    denominator = denominator * rescale + jnp.sum(exponent, -1)
    update = jnp.einsum(
        "hqk,khe->qhe",
        exponent.astype(jnp.bfloat16),
        keyval_heads[..., NOPE:],
        preferred_element_type=jnp.float32,
    )
    accumulated = accumulated * rescale.T[..., None] + update
    final_state = (new_high, denominator, accumulated)
    denominator = final_state[1]
    accumulated = final_state[2]
    attended = (
        (accumulated / denominator.T[..., None])
        .astype(jnp.bfloat16)
        .reshape(first_rows, head_count * VDIM)
    )
    mixture = sent_and_summed(
        jnp.dot(attended, output_weight, preferred_element_type=jnp.float32).astype(jnp.bfloat16),
        "tp",
        0,
    )
    mixed = rms_scale(mixture, output_gain)
    tok_rows = second_rows.shape[0]
    model_width = second_rows.shape[1]
    top_count = route_ids.shape[1]
    local_count = gate_weight.shape[0]
    expert_count = local_count * ep_count
    capacity = max(tp_count, tok_rows * top_count * 2 // expert_count // tp_count * tp_count)
    normed = rms_scale(second_rows, second_gain)
    flat_ids = route_ids.reshape(-1)
    onehot = (flat_ids[:, None] == jnp.arange(expert_count, dtype=jnp.int32)[None, :]).astype(
        jnp.int32
    )
    slot_rank = jnp.sum((jnp.cumsum(onehot, 0) - 1) * onehot, 1)
    owners = jnp.arange(tok_rows * top_count, dtype=jnp.int32) // top_count
    slot_table = (
        jnp.full((expert_count * capacity,), tok_rows, jnp.int32)
        .at[flat_ids * capacity + slot_rank]
        .set(owners)
    )
    padded = jnp.concatenate([normed, jnp.zeros((1, model_width), jnp.bfloat16)], 0)
    outgoing = padded[slot_table].reshape(ep_count, local_count, capacity, model_width)
    weights = route_weights.reshape(-1, 1)
    shared_hidden = (
        jax.nn.silu(jnp.dot(normed, shared_gate, preferred_element_type=jnp.float32))
        * jnp.dot(normed, shared_up, preferred_element_type=jnp.float32)
    ).astype(jnp.bfloat16)
    shared_part = jnp.dot(shared_hidden, shared_down, preferred_element_type=jnp.float32)
    arrived = lax.all_to_all(outgoing, "ep", split_axis=0, concat_axis=0, tiled=True)
    gate_act = jnp.einsum(
        "sicd,idf->sicf", arrived, gate_weight, preferred_element_type=jnp.float32
    )
    up_act = jnp.einsum("sicd,idf->sicf", arrived, up_weight, preferred_element_type=jnp.float32)
    hidden = (jax.nn.silu(gate_act) * up_act).astype(jnp.bfloat16)
    slot_terms = jnp.einsum(
        "sicf,ifd->sicd", hidden, down_weight, preferred_element_type=jnp.float32
    ).reshape(-1, model_width)
    slot_sum, shared_sum = (
        lax.psum_scatter(
            slot_terms.astype(jnp.bfloat16), "tp", scatter_dimension=1, tiled=True
        ).astype(jnp.float32),
        lax.psum_scatter(
            shared_part.astype(jnp.bfloat16), "tp", scatter_dimension=1, tiled=True
        ).astype(jnp.float32),
    )
    column_part = model_width // tp_count
    returned = lax.all_to_all(
        slot_sum.astype(jnp.bfloat16).reshape(ep_count, local_count * capacity, column_part),
        "ep",
        split_axis=0,
        concat_axis=0,
        tiled=True,
    )
    returned = returned.reshape(expert_count * capacity, column_part)
    picked = returned[flat_ids * capacity + slot_rank].astype(jnp.float32) * weights
    routed = jnp.sum(picked.reshape(tok_rows, top_count, column_part), 1)
    expert_mix = (routed + shared_sum).astype(jnp.bfloat16)
    return (mixed, expert_mix)


def solution(mesh):
    placed = (
        P("ep", None),
        P("ep", None),
        P("ep", None),
        P(),
        P(),
        P(None, "tp"),
        P(None, "tp"),
        P("tp", None),
        P(),
        P("ep", None),
        P(),
        P("ep", None),
        P("ep", None),
        P("ep", None, "tp"),
        P("ep", None, "tp"),
        P("ep", "tp", None),
        P(None, "tp"),
        P(None, "tp"),
        P("tp", None),
    )
    return jax.shard_map(
        per_device,
        mesh=mesh,
        in_specs=placed,
        out_specs=(P(("ep", "tp"), None), P("ep", "tp")),
        check_vma=False,
    )
```

profile of v0, /device:TPU:1, one launch (start us, length us, event | category | flops | bytes accessed | tf_op | source)
XLA Modules:
  0.0 296.7 jit_solution(14478941307192723457)
XLA Ops:
  8.0 0.0 copy-start
  8.0 0.0 all-gather.2.cloned.1.call-start
  8.1 0.8 convert_element_type.93
  8.9 0.1 multiply_cosine_fusion
  9.0 0.1 copy.60
  9.1 0.1 copy.61
  9.2 1.0 fusion.67
  10.3 1.4 convolution_convert_fusion.3
  11.7 0.7 pad_maximum_fusion
  12.4 0.0 all-gather.2.cloned.1.call-update
  12.4 0.0 reduce-scatter.3.cloned.1.call-start
  12.5 0.8 copy.67
  13.3 0.1 eq.29
  13.4 0.1 eq.25
  13.5 1.2 reduce-window.6
  14.7 0.2 slice_reduce_fusion
  15.0 0.7 broadcast_multiply_fusion
  15.7 0.1 copy.66
  15.8 0.1 mul.238
  15.9 0.1 fusion.76
  16.1 2.4 scatter_custom_fusion
  18.5 1.2 fusion.51
  19.7 1.2 fusion.53
  21.1 6.0 %gather_fusion = bf16[1024,2048]{1,0:T(8,128)(2,1)} fusion(bf16[129,2048]{1,0:T(8,128)(2,1)S(1)} %concatenate.16, s32[1024]{0:T(1024)S(1)} %fusion.89), kind=kCustom, calls=%fused_computation | custom fusion | bytes 8392704 | tf_op jit(solution)/shard_map/gather | solution.py:159
  27.1 135.6 %all_to_all.15 = bf16[64,1,16,2048]{3,2,1,0:T(8,128)(2,1)S(1)} all-to-all(bf16[64,1,16,2048]{3,2,1,0:T(8,128)(2,1)} %bitcast.120), channel_id=1, replica_groups=mesh['ep'=64,'tp'=4] {'ep'}, dimensions={0} | all-to-all | bytes 8388608 | tf_op jit(solution)/shard_map/all_to_all | solution.py:166
  162.7 2.1 copy-done.3
  164.8 0.0 copy-done.10
  164.8 2.2 fusion.13
  167.0 0.0 copy-done
  167.0 9.2 %convolution_convert_fusion = bf16[64,16,2048]{2,1,0:T(8,128)(2,1)} fusion(bf16[64,1,16,2048]{3,2,1,0:T(8,128)(2,1)} %copy-done.3, bf16[1,256,2048]{2,1,0:T(8,128)(2,1)S(1)} %copy-done, bf16[1,2048,256]{2,1,0:T(8,128)(2,1)} %param.33, f32[64,1,16,256]{3,2,0,1:T(8,128)} %fusion.13), kind=kOutput, calls=%fused_computation.16 | convolution fusion | flops 2151153664 | bytes 11534336 | tf_op jit(solution)/shard_map/sicf,ifd->sicd/dot_general | solution.py:172
  176.2 0.0 reduce-scatter.3.cloned.1.call-update
  176.2 0.1 fusion.64
  176.4 0.0 copy-done.6
  176.4 0.4 fusion.70
  176.8 0.0 all-gather.2.cloned.1.call-done
  176.9 7.1 %slice.58 = bf16[8192,512]{1,0:T(8,128)(2,1)} slice(bf16[8192,544]{1,0:T(8,128)(2,1)} %all-gather.2.cloned.1.call-done), slice={[0:8192], [0:512]} | slice | bytes 16777216 | tf_op jit(solution)/shard_map/slice | solution.py:19
  184.0 11.8 %copy.76 = bf16[8192,512]{0,1:T(8,128)(2,1)} copy(bf16[8192,512]{1,0:T(8,128)(2,1)} %slice.58) | data formatting | bytes 16777216 | tf_op jit(solution)/shard_map/reshape | solution.py:107
  195.8 9.9 %fusion.12 = f32[8192,128,4]{0,1,2:T(8,128)} fusion(bf16[8192,544]{1,0:T(8,128)(2,1)} %all-gather.2.cloned.1.call-done, bf16[128,4,16]{0,2,1:T(8,128)(2,1)S(1)} %get-tuple-element.3, bf16[128,4,16]{0,2,1:T(8,128)(2,1)S(1)} %get-tuple-element.2), kind=kOutput, calls=%fused_computation.20 | convolution fusion | flops 268500992 | bytes 18907136 | tf_op jit(solution)/shard_map/qhr,kr->hqk/dot_general | solution.py:113
  205.7 10.8 %fusion.98 = (f32[4,128]{1,0:T(4,128)S(1)}, f32[4,128,8192]{2,1,0:T(8,128)}) fusion(f32[8192,128,4]{0,1,2:T(8,128)} %fusion.12, bf16[8192,4,128]{0,2,1:T(8,128)(2,1)S(1)} %bitcast.118, f32[128,4,96]{0,2,1:T(8,128)S(1)} %bitcast.123), kind=kOutput, calls=%fused_computation.117 | convolution fusion | flops 549453312 | bytes 37816320 | tf_op jit(solution)/shard_map/qhd,khd->hqk/dot_general | solution.py:108
  216.5 8.3 %fusion.1 = f32[4,128]{1,0:T(4,128)S(1)} fusion(f32[4,128,8192]{2,1,0:T(8,128)} %get-tuple-element.11, f32[4,128]{1,0:T(4,128)S(1)} %get-tuple-element.10), kind=kLoop, calls=%fused_computation.6 | loop fusion | flops 8388096 | bytes 16781312 | tf_op jit(solution)/shard_map/reduce_sum | solution.py:118
  224.8 0.0 copy-start.4
  224.8 10.2 %fusion.46 = bf16[128,4,64]{0,2,1:T(8,128)(2,1)S(1)} fusion(f32[4,128,8192]{2,1,0:T(8,128)} %get-tuple-element.11, f32[4,128]{1,0:T(4,128)S(1)} %get-tuple-element.10, bf16[8192,4,128]{0,2,1:T(8,128)(2,1)} %bitcast.117, f32[128,4]{0,1:T(4,128)S(1)} %bitcast_add_fusion.1, f32[128,4]{0,1:T(4,128)S(1)} %multiply_bitcast_fusion), kind=kOutput, calls=%fused_computation.34 | convolution fusion | flops 545357824 | bytes 21043200 | tf_op jit(solution)/shard_map/hqk,khe->qhe/dot_general | solution.py:119
  235.0 0.0 copy-start.9
  235.0 0.0 copy-start.7
  235.1 0.0 copy-start.1
  235.1 1.1 convolution_convert_fusion.2
  236.2 4.0 %all-to-all-start = ((bf16[4,32,2048]{2,1,0:T(8,128)(2,1)}), bf16[4,32,2048]{2,1,0:T(8,128)(2,1)S(1)}, u32[]{:S(2)}, u32[]{:S(2)}) async-start(bf16[4,32,2048]{2,1,0:T(8,128)(2,1)} %bitcast.7), calls=%async_computation | async-start | bytes 1048576 | tf_op jit(solution)/shard_map/all_to_all | solution.py:32
  240.2 8.3 %all-to-all-done = bf16[4,32,2048]{2,1,0:T(8,128)(2,1)S(1)} async-done(((bf16[4,32,2048]{2,1,0:T(8,128)(2,1)}), bf16[4,32,2048]{2,1,0:T(8,128)(2,1)S(1)}, u32[]{:S(2)}, u32[]{:S(2)}) %all-to-all-start) | async-done | bytes 524320 | tf_op jit(solution)/shard_map/all_to_all | solution.py:32
  248.5 8.0 %all-to-all-start.2 = ((bf16[64,16,512]{2,1,0:T(8,128)(2,1)}), bf16[64,16,512]{2,1,0:T(8,128)(2,1)S(1)}, u32[]{:S(2)}, u32[]{:S(2)}) async-start(bf16[64,16,512]{2,1,0:T(8,128)(2,1)} %bitcast.124), calls=%async_computation.3 | async-start | bytes 2097152 | tf_op jit(solution)/shard_map/all_to_all | solution.py:184
  256.4 0.0 reduce-scatter.5.cloned.1.call-start
  256.5 1.3 fusion.99
  257.8 2.5 convolution_convert_fusion.1
  260.4 0.0 reduce-scatter.5.cloned.1.call-update
  260.4 0.1 copy.71
  260.5 0.1 convert_reduce_fusion
  260.6 0.1 multiply_reduce_fusion.1
  260.7 0.0 copy-done.7
  260.7 0.8 multiply_convert_fusion
  261.5 23.1 %all-to-all-done.2 = bf16[64,16,512]{2,1,0:T(8,128)(2,1)S(1)} async-done(((bf16[64,16,512]{2,1,0:T(8,128)(2,1)}), bf16[64,16,512]{2,1,0:T(8,128)(2,1)S(1)}, u32[]{:S(2)}, u32[]{:S(2)}) %all-to-all-start.2) | async-done | bytes 1048608 | tf_op jit(solution)/shard_map/all_to_all | solution.py:184
  284.6 2.0 gather_fusion.1
  286.6 0.3 reshape.215
  286.9 0.7 multiply_reduce_fusion
  287.6 0.0 reduce-scatter.5.cloned.1.call-done
  287.7 1.6 add_convert_fusion
  (30 shorter events, 0.2 us)
Async XLA Ops:
  8.0 159.0 %copy-start = (bf16[1,256,2048]{2,1,0:T(8,128)(2,1)S(1)}, bf16[1,256,2048]{2,1,0:T(8,128)(2,1)}, u32[]{:S(2)}) copy-start(bf16[1,256,2048]{2,1,0:T(8,128)(2,1)} %param.34) | copy-start | bytes 3145732
  8.0 168.8 %all-gather.2.cloned.1.call-start = ((), (), s32[]{:S(2)}) async-start(), calls=%async_computation.5 | async-start | bytes 10649600 | tf_op jit(solution)/shard_map/all_gather | solution.py:17
  12.4 227.7 %reduce-scatter.3.cloned.1.call-start = ((), (), s32[]{:S(2)}) async-start(), calls=%async_computation.6 | async-start | bytes 5242880 | tf_op jit(solution)/shard_map/reduce_scatter | solution.py:176
  27.1 137.7 %copy-start.10 = (bf16[1,2048,256]{2,1,0:T(8,128)(2,1)S(1)}, bf16[1,2048,256]{2,1,0:T(8,128)(2,1)}, u32[]{:S(2)}) copy-start(bf16[1,2048,256]{2,1,0:T(8,128)(2,1)} %param.32) | copy-start | bytes 3145732
  162.7 2.1 copy-start.3
  167.0 9.2 %copy-start.5 = (bf16[128,768]{1,0:T(8,128)(2,1)S(1)}, bf16[128,768]{1,0:T(8,128)(2,1)}, u32[]{:S(2)}) copy-start(bf16[128,768]{1,0:T(8,128)(2,1)} %param.19) | copy-start | bytes 589828
  167.0 9.3 %copy-start.6 = (bf16[768,384]{1,0:T(8,128)(2,1)S(1)}, bf16[768,384]{1,0:T(8,128)(2,1)}, u32[]{:S(2)}) copy-start(bf16[768,384]{1,0:T(8,128)(2,1)} %param.24) | copy-start | bytes 1769476
  167.0 9.3 %copy-start.8 = (f32[768]{0:T(1024)S(1)}, f32[768]{0:T(1024)}, u32[]{:S(2)}) copy-start(f32[768]{0:T(1024)} %param.22) | copy-start | bytes 9220
  195.8 9.9 %copy-start.2 = (bf16[8192,512]{0,1:T(8,128)(2,1)S(1)}, bf16[8192,512]{0,1:T(8,128)(2,1)}, u32[]{:S(2)}) copy-start(bf16[8192,512]{0,1:T(8,128)(2,1)} %copy.76) | copy-start | bytes 25165828
  224.8 10.3 %copy-start.4 = (bf16[256,2048]{1,0:T(8,128)(2,1)S(1)}, bf16[256,2048]{1,0:T(8,128)(2,1)}, u32[]{:S(2)}) copy-start(bf16[256,2048]{1,0:T(8,128)(2,1)} %param.26) | copy-start | bytes 3145732
  235.0 25.4 %copy-start.9 = (f32[128,4]{0,1:T(4,128)S(1)}, f32[128,4]{0,1:T(4,128)}, u32[]{:S(2)}) copy-start(f32[128,4]{0,1:T(4,128)} %param.31) | copy-start | bytes 6148
  235.0 25.7 %copy-start.7 = (f32[2048]{0:T(1024)S(1)}, f32[2048]{0:T(1024)}, u32[]{:S(2)}) copy-start(f32[2048]{0:T(1024)} %param.27) | copy-start | bytes 24580
  235.1 54.2 %copy-start.1 = (bf16[1,256,2048]{2,1,0:T(8,128)(2,1)S(1)}, bf16[1,256,2048]{2,1,0:T(8,128)(2,1)}, u32[]{:S(2)}) copy-start(bf16[1,256,2048]{2,1,0:T(8,128)(2,1)} %param.34) | copy-start | bytes 3145732
  236.2 12.3 %all-to-all-start = ((bf16[4,32,2048]{2,1,0:T(8,128)(2,1)}), bf16[4,32,2048]{2,1,0:T(8,128)(2,1)S(1)}, u32[]{:S(2)}, u32[]{:S(2)}) async-start(bf16[4,32,2048]{2,1,0:T(8,128)(2,1)} %bitcast.7), calls=%async_computation | async-start | bytes 1048576 | tf_op jit(solution)/shard_map/all_to_all | solution.py:32
  248.5 36.1 %all-to-all-start.2 = ((bf16[64,16,512]{2,1,0:T(8,128)(2,1)}), bf16[64,16,512]{2,1,0:T(8,128)(2,1)S(1)}, u32[]{:S(2)}, u32[]{:S(2)}) async-start(bf16[64,16,512]{2,1,0:T(8,128)(2,1)} %bitcast.124), calls=%async_computation.3 | async-start | bytes 2097152 | tf_op jit(solution)/shard_map/all_to_all | solution.py:184
  256.4 31.2 %reduce-scatter.5.cloned.1.call-start = ((), (), s32[]{:S(2)}) async-start(), calls=%async_computation.7 | async-start | bytes 655360 | tf_op jit(solution)/shard_map/reduce_scatter | solution.py:179
Sparse Core Ops, SparseCore 0:
  12.6 147.9 all-gather.1
Sparse Core Ops, SparseCore 1:
  176.3 46.5 reduce-scatter.2
  260.5 21.1 reduce-scatter.4
where the time goes:
time: 298 us; the launch traced here: 297 us
  blocking collectives  136 us (46%)
  matrix products  49.1 us (16%)
  local copies, waits for them, and re-layouts  33.7 us (11%)
  waiting for transfers between devices  31.5 us (11%)
  other arithmetic  18.9 us (6%)
  between operations  15.7 us (5%)
  starting transfers between devices  12.1 us (4%)
    all_to_all x1, blocking collectives, per_device(): lax.all_to_all(outgoing, 'ep', split_axis=0, concat_axis=0, tiled=True)  136 us
    all_to_all x1, waiting for transfers between devices, per_device(): lax.all_to_all(slot_sum.astype(jnp.bfloat16).reshape(ep_count, local_coun...  23.1 us
    reshape x1, local copies, waits for them, and re-layouts, per_device(): keyval_heads = keyval_piece.reshape(key_count, head_count, NOPE + VDIM)  11.8 us
    dot_general x1, matrix products, per_device(): jnp.einsum('qhd,khd->hqk', query_plain, keyval_heads[..., :NOPE], preferr...  10.8 us
    dot_general x1, matrix products, per_device(): jnp.einsum('hqk,khe->qhe', exponent.astype(jnp.bfloat16), keyval_heads[.....  10.2 us
    dot_general x1, matrix products, per_device(): jnp.einsum('qhr,kr->hqk', query_turned, rot_piece, preferred_element_type...  9.87 us
    dot_general x1, matrix products, per_device(): jnp.einsum('sicf,ifd->sicd', hidden, down_weight, preferred_element_type=...  9.16 us
    all_to_all x1, waiting for transfers between devices, sent_and_summed(): lax.all_to_all(pieces, axis, split_axis=0, concat_axis=0, tiled=True)  8.3 us
  transfers between devices with their start and end apart: 5, of which 2 were waited for; matrix products, arithmetic and copies ran while one was open for 32% of the time, Pallas kernels for 0%

commit v1 on v0

v1 whole, which is shorter than its diff:
```python
import functools

import jax
import jax.numpy as jnp
from jax import lax
from jax.experimental import pallas as pl
from jax.experimental.pallas import tpu as pltpu
from jax.sharding import PartitionSpec as P

NOPE = 64
ROPE = 32
VDIM = 64
EPS = 1e-06
ROPE_BASE = 10000.0
MESH = pl.DeviceIdType.MESH
F32 = jnp.float32
BF16 = jnp.bfloat16


def rms_scale(values, gain_vec):
    widened = values.astype(jnp.float32)
    normed = widened * lax.rsqrt(jnp.mean(widened * widened, -1, keepdims=True) + EPS)
    return (normed * gain_vec).astype(jnp.bfloat16)


def rotate(values, positions):
    half_width = values.shape[-1] // 2
    inverse = 1.0 / ROPE_BASE ** (
        jnp.arange(half_width, dtype=jnp.float32) * 2.0 / (2 * half_width)
    )
    angles = positions[:, None] * inverse[None, :]
    cosine = jnp.cos(angles)
    sine_vals = jnp.sin(angles)
    if values.ndim == 3:
        cosine = cosine[:, None, :]
        sine_vals = sine_vals[:, None, :]
    first_half = values[..., :half_width]
    second = values[..., half_width:]
    return jnp.concatenate(
        [first_half * cosine - second * sine_vals, first_half * sine_vals + second * cosine], -1
    )


def cut_along(shard, dim, size):
    lengths = shard.shape
    pieces = shard.reshape(*lengths[:dim], size, lengths[dim] // size, *lengths[dim + 1 :])
    return jnp.moveaxis(pieces, dim, 0)


def sent_and_summed(shard, axis, dim):
    pieces = cut_along(shard, dim, lax.axis_size(axis))
    arrived = lax.all_to_all(pieces, axis, split_axis=0, concat_axis=0, tiled=True)
    return arrived.astype(jnp.float32).sum(axis=0)


def mm(a, b):
    return jnp.dot(a, b, preferred_element_type=F32)


def iota(shape, dim):
    return lax.broadcasted_iota(jnp.int32, shape, dim)


NCH = 8
ROWS = 128
COLS = 512


def moe_kernel(
    rows_ref, gain_ref, ids_ref, idst_ref, w_ref,
    wg_hbm, wu_hbm, wd_hbm, sg_hbm, su_hbm, sd_hbm,
    out_ref,
    nrm, outq, wg, wu, wd, sg, su, sd, chi, clo,
    held, part, rly, fin, ret, back, acc,
    w_sem, disp_send, disp_recv, ag_send, agr, agl, agrr, agrl,
    rs_send, rlyr, rlyl, finr, finl, ret_send, ret_recv,
):
    e = lax.axis_index("ep")
    t = lax.axis_index("tp")
    z = e // 8
    k0 = e % 8
    right = (t + 1) % 4
    left = (t + 3) % 4
    opp = (t + 2) % 4

    barrier = pltpu.get_barrier_semaphore()

    def greet(j, _):
        pl.semaphore_signal(
            barrier, inc=1, device_id={"ep": (e + j) % 64, "tp": t}, device_id_type=MESH
        )
        return 0

    lax.fori_loop(1, 64, greet, 0)
    for other in (right, left):
        pl.semaphore_signal(barrier, inc=1, device_id={"ep": e, "tp": other}, device_id_type=MESH)

    loads = [
        pltpu.make_async_copy(src, dst, w_sem.at[n])
        for n, (src, dst) in enumerate(
            ((sg_hbm, sg), (su_hbm, su), (sd_hbm, sd), (wg_hbm, wg), (wu_hbm, wu), (wd_hbm, wd))
        )
    ]
    for load in loads:
        load.start()

    x = rows_ref[...].astype(F32)
    scale = lax.rsqrt(jnp.mean(x * x, -1, keepdims=True) + EPS)
    nrm[...] = (x * scale * gain_ref[...]).astype(BF16)

    idst = idst_ref[...]
    member_t = jnp.zeros((64, ROWS), F32)
    for k in range(4):
        member_t = member_t + jnp.where(idst[k : k + 1, :] == iota((64, ROWS), 0), 1.0, 0.0)
    before = jnp.where(iota((ROWS, ROWS), 0) < iota((ROWS, ROWS), 1), 1.0, 0.0).astype(BF16)
    place_t = (member_t * (mm(member_t.astype(BF16), before) + 1.0)).astype(BF16)
    spread_t = jnp.where((iota((1024, 64), 0) >> 4) == iota((1024, 64), 1), 1.0, 0.0).astype(BF16)
    slot_t = ((iota((1024, ROWS), 0) & 15) + 1).astype(F32)
    pick = jnp.where(mm(spread_t, place_t) == slot_t, 1.0, 0.0).astype(BF16)
    own_cols = pl.ds(pl.multiple_of(t * COLS, COLS), COLS)
    outq[...] = mm(pick, nrm[:, own_cols]).astype(BF16)

    pl.semaphore_wait(barrier, 65)

    def rows16(k):
        return pl.ds(pl.multiple_of(k * 16, 16), 16)

    def dispatch(n, _):
        i, k = n // 8, n % 8
        dest = ((z + 8 - i) % 8) * 8 + k

        @pl.when(dest != e)
        def _():
            pltpu.make_async_remote_copy(
                src_ref=outq.at[rows16(dest)],
                dst_ref=held.at[i, t, rows16(k0)],
                send_sem=disp_send,
                recv_sem=disp_recv.at[i],
                device_id={"ep": dest, "tp": t},
                device_id_type=MESH,
            ).start()

        return 0

    lax.fori_loop(0, 64, dispatch, 0)
    held[0, t, rows16(k0)] = outq[rows16(e)]

    ids = ids_ref[...]
    wts = w_ref[...]
    member = jnp.zeros((ROWS, 64), F32)
    weight = jnp.zeros((ROWS, 64), F32)
    for k in range(4):
        hit = ids[:, k : k + 1] == iota((ROWS, 64), 1)
        member = member + jnp.where(hit, 1.0, 0.0)
        weight = weight + jnp.where(hit, wts[:, k : k + 1], 0.0)
    after = jnp.where(iota((ROWS, ROWS), 0) > iota((ROWS, ROWS), 1), 1.0, 0.0).astype(BF16)
    place = (member * (mm(after, member.astype(BF16)) + 1.0)).astype(BF16)
    spread = jnp.where((iota((64, 1024), 1) >> 4) == iota((64, 1024), 0), 1.0, 0.0).astype(BF16)
    slot = ((iota((ROWS, 1024), 1) & 15) + 1).astype(F32)
    chosen = mm(place, spread) == slot
    high = weight.astype(BF16)
    low = (weight - high.astype(F32)).astype(BF16)
    chi[...] = jnp.where(chosen, mm(high, spread), 0.0).astype(BF16)
    clo[...] = jnp.where(chosen, mm(low, spread), 0.0).astype(BF16)

    def side(src, dst, send_sem, recv_sem, other):
        return pltpu.make_async_remote_copy(
            src_ref=src, dst_ref=dst, send_sem=send_sem, recv_sem=recv_sem,
            device_id={"ep": e, "tp": other}, device_id_type=MESH,
        )

    lo_half = pl.ds(0, 64)
    hi_half = pl.ds(64, 64)

    def scatter_first(n):
        side(part.at[n, opp, lo_half], rly.at[n, 0], rs_send, rlyr.at[n], right).start()
        side(part.at[n, opp, hi_half], rly.at[n, 1], rs_send, rlyl.at[n], left).start()
        side(part.at[n, right, hi_half], fin.at[n, 0, hi_half], rs_send, finr.at[n], right).start()
        side(part.at[n, left, lo_half], fin.at[n, 1, lo_half], rs_send, finl.at[n], left).start()

    def scatter_second(n):
        side(rly.at[n, 0], rly.at[n, 0], rs_send, rlyr.at[n], right).wait_recv()
        part[n, right, lo_half] = (
            part[n, right, lo_half].astype(F32) + rly[n, 0].astype(F32)
        ).astype(BF16)
        side(part.at[n, right, lo_half], fin.at[n, 0, lo_half], rs_send, finr.at[n], right).start()
        side(rly.at[n, 1], rly.at[n, 1], rs_send, rlyl.at[n], left).wait_recv()
        part[n, left, hi_half] = (
            part[n, left, hi_half].astype(F32) + rly[n, 1].astype(F32)
        ).astype(BF16)
        side(part.at[n, left, hi_half], fin.at[n, 1, hi_half], rs_send, finl.at[n], left).start()

    def scatter_last(n):
        side(fin.at[n, 0], fin.at[n, 0], rs_send, finr.at[n], right).wait_recv()
        side(fin.at[n, 1], fin.at[n, 1], rs_send, finl.at[n], left).wait_recv()
        return part[n, t].astype(F32) + fin[n, 0].astype(F32) + fin[n, 1].astype(F32)

    def swish(g, u):
        return (g / (1.0 + jnp.exp(-g)) * u).astype(BF16)

    for load in loads[:3]:
        load.wait()
    shared = swish(mm(nrm[...], sg[...]), mm(nrm[...], su[...]))
    for q in range(4):
        part[NCH, q] = mm(shared, sd[:, q * COLS : (q + 1) * COLS]).astype(BF16)
    scatter_first(NCH)
    for load in loads[3:]:
        load.wait()

    acc[...] = jnp.zeros_like(acc)

    def arrive(i):
        @pl.when(i == 0)
        def _():
            some = held.at[0, t, pl.ds(0, 112)]
            side(some, some, disp_send, disp_recv.at[0], right).wait_recv()

        @pl.when(i > 0)
        def _():
            whole = held.at[i, t]
            side(whole, whole, disp_send, disp_recv.at[i], right).wait_recv()

        side(held.at[i, t], held.at[i, t], ag_send, agr.at[i], right).start()
        side(held.at[i, t], held.at[i, t], ag_send, agl.at[i], left).start()

    def pass_on(i):
        side(held.at[i, left], held.at[i, left], ag_send, agr.at[i], right).wait_recv()
        side(
            held.at[i, left, lo_half], held.at[i, left, lo_half], ag_send, agrr.at[i], right
        ).start()
        side(held.at[i, right], held.at[i, right], ag_send, agl.at[i], left).wait_recv()
        side(
            held.at[i, right, hi_half], held.at[i, right, hi_half], ag_send, agrl.at[i], left
        ).start()

    def expert(i):
        side(
            held.at[i, opp, lo_half], held.at[i, opp, lo_half], ag_send, agrr.at[i], right
        ).wait_recv()
        side(
            held.at[i, opp, hi_half], held.at[i, opp, hi_half], ag_send, agrl.at[i], left
        ).wait_recv()
        g = jnp.zeros((ROWS, 256), F32)
        u = jnp.zeros((ROWS, 256), F32)
        for q in range(4):
            piece = held[i, q]
            g = g + mm(piece, wg[q * COLS : (q + 1) * COLS, :])
            u = u + mm(piece, wu[q * COLS : (q + 1) * COLS, :])
        hidden = swish(g, u)
        for q in range(4):
            part[i, q] = mm(hidden, wd[:, q * COLS : (q + 1) * COLS]).astype(BF16)
        scatter_first(i)

    def give_back(i):
        ret[i] = scatter_last(i).astype(BF16)

        def one(k, _):
            dest = ((z + i) % 8) * 8 + k

            @pl.when(dest != e)
            def _():
                pltpu.make_async_remote_copy(
                    src_ref=ret.at[i, rows16(k)],
                    dst_ref=back.at[i, rows16(k0)],
                    send_sem=ret_send,
                    recv_sem=ret_recv.at[i],
                    device_id={"ep": dest, "tp": t},
                    device_id_type=MESH,
                ).start()

            return 0

        lax.fori_loop(0, 8, one, 0)

        @pl.when(i == 0)
        def _():
            back[0, rows16(k0)] = ret[0, rows16(k0)]

    def combine(i):
        @pl.when(i == 0)
        def _():
            some = back.at[0, pl.ds(0, 112)]
            side(some, some, ret_send, ret_recv.at[0], right).wait_recv()

        @pl.when(i > 0)
        def _():
            side(back.at[i], back.at[i], ret_send, ret_recv.at[i], right).wait_recv()

        cols = pl.ds(pl.multiple_of(((z + 8 - i) % 8) * 128, 128), 128)
        acc[...] += mm(chi[:, cols], back[i]) + mm(clo[:, cols], back[i])

    def step(j, _):
        for stage, lag in (
            (arrive, 0), (pass_on, 1), (expert, 2), (scatter_second, 3), (give_back, 4), (combine, 5)
        ):
            @pl.when(jnp.logical_and(j >= lag, j < lag + NCH))
            def _(stage=stage, lag=lag):
                stage(j - lag)

        @pl.when(j == 1)
        def _():
            scatter_second(NCH)

        @pl.when(j == 3)
        def _():
            acc[...] += scatter_last(NCH)

        return 0

    lax.fori_loop(0, NCH + 5, step, 0)
    out_ref[...] = acc[...].astype(BF16)

    sent = outq.at[pl.ds(0, 1008)]
    side(sent, sent, disp_send, disp_recv.at[0], right).wait_send()

    def drain(i, _):
        for piece in (held.at[i, 0], held.at[i, 0], held.at[i, 0]):
            side(piece, piece, ag_send, agr.at[0], right).wait_send()
        return 0

    lax.fori_loop(0, NCH, drain, 0)

    def drain_rs(n, _):
        for piece in (part.at[n, 0], part.at[n, 0], part.at[n, 0]):
            side(piece, piece, rs_send, finr.at[0], right).wait_send()
        return 0

    lax.fori_loop(0, NCH + 1, drain_rs, 0)
    for i in range(NCH):
        piece = ret.at[i, pl.ds(0, 112 if i == 0 else 128)]
        side(piece, piece, ret_send, ret_recv.at[0], right).wait_send()


def moe(rows, gain, ids, wts, wg, wu, wd, sg, su, sd):
    vm = pl.BlockSpec(memory_space=pltpu.VMEM)
    anym = pl.BlockSpec(memory_space=pl.ANY)
    dma = pltpu.SemaphoreType.DMA
    return pl.pallas_call(
        moe_kernel,
        name="moe",
        out_shape=jax.ShapeDtypeStruct((ROWS, COLS), BF16),
        in_specs=[vm] * 5 + [anym] * 6,
        out_specs=vm,
        scratch_shapes=[
            pltpu.VMEM((ROWS, 2048), BF16),
            pltpu.VMEM((1024, COLS), BF16),
            pltpu.VMEM((2048, 256), BF16),
            pltpu.VMEM((2048, 256), BF16),
            pltpu.VMEM((256, 2048), BF16),
            pltpu.VMEM((2048, 128), BF16),
            pltpu.VMEM((2048, 128), BF16),
            pltpu.VMEM((128, 2048), BF16),
            pltpu.VMEM((ROWS, 1024), BF16),
            pltpu.VMEM((ROWS, 1024), BF16),
            pltpu.VMEM((NCH, 4, ROWS, COLS), BF16),
            pltpu.VMEM((NCH + 1, 4, ROWS, COLS), BF16),
            pltpu.VMEM((NCH + 1, 2, 64, COLS), BF16),
            pltpu.VMEM((NCH + 1, 2, ROWS, COLS), BF16),
            pltpu.VMEM((NCH, ROWS, COLS), BF16),
            pltpu.VMEM((NCH, ROWS, COLS), BF16),
            pltpu.VMEM((ROWS, COLS), F32),
            dma((6,)),
            dma, dma((NCH,)),
            dma, dma((NCH,)), dma((NCH,)), dma((NCH,)), dma((NCH,)),
            dma, dma((NCH + 1,)), dma((NCH + 1,)), dma((NCH + 1,)), dma((NCH + 1,)),
            dma, dma((NCH,)),
        ],
        compiler_params=pltpu.CompilerParams(
            collective_id=0, has_side_effects=True, vmem_limit_bytes=56 * 1024 * 1024
        ),
        cost_estimate=pl.CostEstimate(flops=80_000_000_000, bytes_accessed=8_000_000, transcendentals=0),
    )(rows, gain.reshape(1, -1), ids, ids.T, wts, wg, wu, wd, sg, su, sd)


def per_device(
    query_latent, keyval_latent, rotary_key, query_gain, keyval_gain, query_weight, keyval_weight,
    output_weight, output_gain, second_rows, second_gain, route_ids, route_weights,
    gate_weight, up_weight, down_weight, shared_gate, shared_up, shared_down,
):
    first_rows = query_latent.shape[0]
    head_count = query_weight.shape[1] // (NOPE + ROPE)
    positions = (lax.axis_index("ep") * first_rows).astype(jnp.float32) + jnp.arange(
        first_rows, dtype=jnp.float32
    )
    queries = jnp.dot(
        rms_scale(query_latent, query_gain), query_weight, preferred_element_type=jnp.float32
    ).reshape(first_rows, head_count, NOPE + ROPE)
    queries = jnp.concatenate(
        [queries[..., :NOPE], rotate(queries[..., NOPE:], positions)], -1
    ).astype(jnp.bfloat16)
    query_plain = queries[..., :NOPE]
    query_turned = queries[..., NOPE:]
    kv_normed = rms_scale(keyval_latent, keyval_gain)
    key_rot = rotate(rotary_key.astype(jnp.float32), positions).astype(jnp.bfloat16)
    score_scale = (NOPE + ROPE) ** (-0.5)
    keyvals = jnp.dot(kv_normed, keyval_weight, preferred_element_type=jnp.float32).astype(
        jnp.bfloat16
    )
    both = lax.all_gather(jnp.concatenate([keyvals, key_rot], 1), "ep", axis=0, tiled=True)
    expert_mix = moe(
        second_rows, second_gain, route_ids, route_weights,
        gate_weight[0], up_weight[0], down_weight[0], shared_gate, shared_up, shared_down,
    )
    keyval_piece = both[:, : keyvals.shape[1]]
    rot_piece = both[:, keyvals.shape[1] :]
    keyval_heads = keyval_piece.reshape(-1, head_count, NOPE + VDIM)
    scores = jnp.einsum(
        "qhd,khd->hqk", query_plain, keyval_heads[..., :NOPE], preferred_element_type=jnp.float32
    )
    scores = (
        scores
        + jnp.einsum("qhr,kr->hqk", query_turned, rot_piece, preferred_element_type=jnp.float32)
    ) * score_scale
    new_high = jnp.max(scores, -1)
    exponent = jnp.exp(scores - new_high[..., None])
    denominator = jnp.sum(exponent, -1)
    accumulated = jnp.einsum(
        "hqk,khe->qhe",
        exponent.astype(jnp.bfloat16),
        keyval_heads[..., NOPE:],
        preferred_element_type=jnp.float32,
    )
    attended = (
        (accumulated / denominator.T[..., None])
        .astype(jnp.bfloat16)
        .reshape(first_rows, head_count * VDIM)
    )
    mixture = sent_and_summed(
        jnp.dot(attended, output_weight, preferred_element_type=jnp.float32).astype(jnp.bfloat16),
        "tp",
        0,
    )
    mixed = rms_scale(mixture, output_gain)
    return (mixed, expert_mix)


def solution(mesh):
    placed = (
        P("ep", None), P("ep", None), P("ep", None), P(), P(), P(None, "tp"), P(None, "tp"),
        P("tp", None), P(), P("ep", None), P(), P("ep", None), P("ep", None),
        P("ep", None, "tp"), P("ep", None, "tp"), P("ep", "tp", None),
        P(None, "tp"), P(None, "tp"), P("tp", None),
    )
    return jax.shard_map(
        per_device,
        mesh=mesh,
        in_specs=placed,
        out_specs=(P(("ep", "tp"), None), P("ep", "tp")),
        check_vma=False,
    )
```

time: 298 us -> 274 us (0.919)
  blocking collectives: 136 us -> 0 us
  Pallas kernels: 0 us -> 99.9 us
  waiting for transfers between devices: 31.5 us -> 84.8 us
  matrix products: 49.1 us -> 34.6 us
  local copies, waits for them, and re-layouts: 33.7 us -> 23.2 us
  starting transfers between devices: 12.1 us -> 4.03 us
  other arithmetic: 18.9 us -> 12.8 us
    all_to_all x1 -> x0, blocking collectives: 136 us -> none  [per_device(): lax.all_to_all(outgoing, 'ep', split_axis=0, concat_axis=0, tiled=True)]
    pallas_call x0 -> x1, Pallas kernels: none -> 99.9 us  [moe(): pl.pallas_call(moe_kernel, name='moe', out_shape=jax.ShapeDtypeStruct((RO...]
    all_gather x1, waiting for transfers between devices: 0.02 us -> 84.8 us  [per_device(): lax.all_gather(jnp.concatenate([keyvals, key_rot], 1), 'ep', axis=0, tile...]
    all_to_all x1 -> x0, waiting for transfers between devices: 23.1 us -> none  [per_device(): lax.all_to_all(slot_sum.astype(jnp.bfloat16).reshape(ep_count, local_coun...]
    dot_general x4 -> x0, matrix products: 15.3 us -> none  [the longest x1 9.16 us: per_device(): jnp.einsum('sicf,ifd->sicd', hidden, down_weight, preferred_element_type=...]
    all_to_all x1, waiting for transfers between devices: 8.3 us -> 0.01 us  [sent_and_summed(): lax.all_to_all(pieces, axis, split_axis=0, concat_axis=0, tiled=True)]
    gather x2 -> x0, local copies, waits for them, and re-layouts: 7.98 us -> none  [the longest x1 6.02 us: per_device(): padded[slot_table].reshape(ep_count, local_count, capacity, model_width)]
    all_to_all x1 -> x0, starting transfers between devices: 7.97 us -> none  [per_device(): lax.all_to_all(slot_sum.astype(jnp.bfloat16).reshape(ep_count, local_coun...]
  transfers between devices with their start and end apart: 5 -> 2, of which waited for: 2 -> 1; matrix products, arithmetic and copies ran while one was open for 32% -> 2% of each run, Pallas kernels for 0% -> 37%
where the time goes in v1:
time: 274 us; the launch traced here: 273 us
  Pallas kernels  99.9 us (36%)
  waiting for transfers between devices  84.8 us (31%)
  matrix products  34.6 us (13%)
  local copies, waits for them, and re-layouts  23.2 us (8%)
  between operations  14.1 us (5%)
  other arithmetic  12.8 us (5%)
  starting transfers between devices  4.03 us (1%)
    pallas_call x1, Pallas kernels, moe(): pl.pallas_call(moe_kernel, name='moe', out_shape=jax.ShapeDtypeStruct((RO...  99.9 us
    all_gather x1, waiting for transfers between devices, per_device(): lax.all_gather(jnp.concatenate([keyvals, key_rot], 1), 'ep', axis=0, tile...  84.8 us
    reshape x1, local copies, waits for them, and re-layouts, per_device(): keyval_heads = keyval_piece.reshape(-1, head_count, NOPE + VDIM)  11.4 us
    dot_general x1, matrix products, per_device(): jnp.einsum('qhd,khd->hqk', query_plain, keyval_heads[..., :NOPE], preferr...  10.4 us
    dot_general x1, matrix products, per_device(): jnp.einsum('hqk,khe->qhe', exponent.astype(jnp.bfloat16), keyval_heads[.....  10.1 us
    dot_general x1, matrix products, per_device(): jnp.einsum('qhr,kr->hqk', query_turned, rot_piece, preferred_element_type...  9.83 us
    reduce_sum x1, other arithmetic, per_device(): denominator = jnp.sum(exponent, -1)  8.11 us
    slice x1, local copies, waits for them, and re-layouts, per_device(): keyval_piece = both[:, :keyvals.shape[1]]  7.14 us
  transfers between devices with their start and end apart: 2, of which 1 were waited for; matrix products, arithmetic and copies ran while one was open for 2% of the time, Pallas kernels for 37%

profile of v1, /device:TPU:1, one launch (start us, length us, event | category | flops | bytes accessed | tf_op | source)
XLA Modules:
  0.0 273.4 jit_solution(5682392385417902284)
XLA Ops:
  7.2 0.0 copy-start
  7.2 0.0 all-gather.2.cloned.1.call-start
  7.2 0.8 convert_element_type.41
  8.0 0.1 multiply_cosine_fusion
  8.2 0.1 copy.43
  8.3 0.1 copy.44
  8.4 1.0 fusion.27
  9.4 1.4 convolution_convert_fusion.1
  10.8 0.7 pad_maximum_fusion
  11.6 0.0 all-gather.2.cloned.1.call-update
  11.6 1.4 copy.50.ids_ref
  13.0 1.4 copy.51.w_ref
  14.4 1.0 fusion.24
  15.5 1.6 fusion.30
  17.1 84.8 %all-gather.2.cloned.1.call-done = bf16[8192,544]{1,0:T(8,128)(2,1)} async-done(((bf16[128,544]{1,0:T(8,128)(2,1)}), bf16[8192,544]{1,0:T(8,128)(2,1)}) %all-gather.2.cloned.1.call-update) | async-done | bytes 8912912 | tf_op jit(solution)/shard_map/all_gather | solution.py:399
  101.9 7.1 %slice.45 = bf16[8192,512]{1,0:T(8,128)(2,1)} slice(bf16[8192,544]{1,0:T(8,128)(2,1)} %all-gather.2.cloned.1.call-done), slice={[0:8192], [0:512]} | slice | bytes 16777216 | tf_op jit(solution)/shard_map/slice | solution.py:404
  109.1 11.4 %copy.56 = bf16[8192,512]{0,1:T(8,128)(2,1)} copy(bf16[8192,512]{1,0:T(8,128)(2,1)} %slice.45) | data formatting | bytes 16777216 | tf_op jit(solution)/shard_map/reshape | solution.py:406
  120.4 0.0 slice-start
  120.4 0.0 slice-start.1
  120.4 9.8 %fusion.8 = f32[8192,128,4]{0,1,2:T(8,128)} fusion(bf16[8192,544]{1,0:T(8,128)(2,1)} %all-gather.2.cloned.1.call-done, bf16[128,4,16]{0,2,1:T(8,128)(2,1)S(1)} %get-tuple-element.3, bf16[128,4,16]{0,2,1:T(8,128)(2,1)S(1)} %get-tuple-element.2), kind=kOutput, calls=%fused_computation.11 | convolution fusion | flops 268500992 | bytes 18907136 | tf_op jit(solution)/shard_map/qhr,kr->hqk/dot_general | solution.py:412
  130.3 0.0 slice-done
  130.3 0.0 slice-done.1
  130.3 10.4 %fusion.41 = (f32[4,128]{1,0:T(4,128)S(1)}, f32[4,128,8192]{2,1,0:T(8,128)}) fusion(f32[8192,128,4]{0,1,2:T(8,128)} %fusion.8, bf16[8192,4,128]{0,2,1:T(8,128)(2,1)S(1)} %bitcast.30, f32[128,4,96]{0,2,1:T(8,128)S(1)} %bitcast.32), kind=kOutput, calls=%fused_computation.51 | convolution fusion | flops 549453312 | bytes 37816320 | tf_op jit(solution)/shard_map/qhd,khd->hqk/dot_general | solution.py:407
  140.7 8.1 %fusion.1 = f32[4,128]{1,0:T(4,128)S(1)} fusion(f32[4,128,8192]{2,1,0:T(8,128)} %get-tuple-element.11, f32[4,128]{1,0:T(4,128)S(1)} %get-tuple-element.10), kind=kLoop, calls=%fused_computation.3 | loop fusion | flops 8388096 | bytes 16781312 | tf_op jit(solution)/shard_map/reduce_sum | solution.py:416
  148.8 10.1 %fusion.19 = bf16[128,4,64]{0,2,1:T(8,128)(2,1)S(1)} fusion(f32[4,128,8192]{2,1,0:T(8,128)} %get-tuple-element.11, f32[4,128]{1,0:T(4,128)S(1)} %get-tuple-element.10, bf16[8192,4,128]{0,2,1:T(8,128)(2,1)} %bitcast.27, f32[128,4]{0,1:T(4,128)S(1)} %bitcast.34), kind=kOutput, calls=%fused_computation.15 | convolution fusion | flops 545325056 | bytes 21041152 | tf_op jit(solution)/shard_map/hqk,khe->qhe/dot_general | solution.py:417
  159.0 0.0 copy-done
  159.0 1.1 convolution_convert_fusion
  160.1 4.0 %all-to-all-start = ((bf16[4,32,2048]{2,1,0:T(8,128)(2,1)}), bf16[4,32,2048]{2,1,0:T(8,128)(2,1)S(1)}, u32[]{:S(2)}, u32[]{:S(2)}) async-start(bf16[4,32,2048]{2,1,0:T(8,128)(2,1)} %bitcast.6), calls=%async_computation | async-start | bytes 1048576 | tf_op jit(solution)/shard_map/all_to_all | solution.py:52
  164.1 0.0 copy-start.2
  164.1 0.0 copy-start.1
  164.1 99.9 %moe.1 = bf16[128,512]{1,0:T(8,128)(2,1)} custom-call(bf16[128,2048]{1,0:T(8,128)(2,1)} %rows_ref.1, f32[1,2048]{1,0:T(1,128)} %bitcast.39, s32[128,4]{1,0:T(8,128)} %copy.50.ids_ref, s32[4,128]{1,0:T(4,128)} %bitcast.35, f32[128,4]{1,0:T(8,128)} %copy.51.w_ref, bf16[2048,256]{1,0:T(8,128)(2,1)} %bitcast.36, bf16[2048,256]{1,0:T(8,128)(2,1)} %bitcast.37, ...), custom_call_target="tpu_custom_call" | custom-call | flops 80000000000 | bytes 8000000 | tf_op jit(solution)/shard_map/moe/pallas_call | solution.py:338
  264.0 0.0 all-to-all-done
  264.0 0.1 convert_reduce_fusion
  264.1 0.1 multiply_reduce_fusion
  264.2 0.0 copy-done.2
  264.2 0.8 multiply_convert_fusion
  265.0 1.6 copy.58
  266.5 0.0 copy-done.1
  (7 shorter events, 0.1 us)
Async XLA Ops:
  7.2 151.8 %copy-start = (bf16[256,2048]{1,0:T(8,128)(2,1)S(1)}, bf16[256,2048]{1,0:T(8,128)(2,1)}, u32[]{:S(2)}) copy-start(bf16[256,2048]{1,0:T(8,128)(2,1)} %param.26) | copy-start | bytes 3145732
  7.2 94.7 %all-gather.2.cloned.1.call-start = ((), (), s32[]{:S(2)}) async-start(), calls=%async_computation.1 | async-start | bytes 10649600 | tf_op jit(solution)/shard_map/all_gather | solution.py:399
  120.4 9.8 %slice-start = ((s8[8388608]{0:T(1024)(128)(4,1)}), s8[4194304]{0:T(1024)(128)(4,1)S(1)}, s32[]{:S(2)}) async-start(s8[8388608]{0:T(1024)(128)(4,1)} %bitcast.28), calls=%async_computation.2 | async-start | bytes 8388608
  120.4 9.8 %slice-start.1 = ((s8[8388608]{0:T(1024)(128)(4,1)}), s8[4194304]{0:T(1024)(128)(4,1)S(1)}, s32[]{:S(2)}) async-start(s8[8388608]{0:T(1024)(128)(4,1)} %bitcast.28), calls=%async_computation.3 | async-start | bytes 8388608
  160.1 103.9 %all-to-all-start = ((bf16[4,32,2048]{2,1,0:T(8,128)(2,1)}), bf16[4,32,2048]{2,1,0:T(8,128)(2,1)S(1)}, u32[]{:S(2)}, u32[]{:S(2)}) async-start(bf16[4,32,2048]{2,1,0:T(8,128)(2,1)} %bitcast.6), calls=%async_computation | async-start | bytes 1048576 | tf_op jit(solution)/shard_map/all_to_all | solution.py:52
  164.1 100.1 %copy-start.2 = (f32[2048]{0:T(1024)S(1)}, f32[2048]{0:T(1024)}, u32[]{:S(2)}) copy-start(f32[2048]{0:T(1024)} %param.27) | copy-start | bytes 24580
  164.1 102.4 %copy-start.1 = (bf16[256,2048]{1,0:T(8,128)(2,1)S(1)}, bf16[256,2048]{1,0:T(8,128)(2,1)}, u32[]{:S(2)}) copy-start(bf16[256,2048]{1,0:T(8,128)(2,1)} %param.26) | copy-start | bytes 3145732
Sparse Core Ops, SparseCore 0:
  11.7 90.1 all-gather.1

commit v2 on v1

v2 whole, which is shorter than its diff:
```python
import functools

import jax
import jax.numpy as jnp
from jax import lax
from jax.experimental import pallas as pl
from jax.experimental.pallas import tpu as pltpu
from jax.sharding import PartitionSpec as P

NOPE = 64
ROPE = 32
VDIM = 64
EPS = 1e-06
ROPE_BASE = 10000.0
MESH = pl.DeviceIdType.MESH
F32 = jnp.float32
BF16 = jnp.bfloat16


def mm(a, b):
    return jnp.dot(a, b, preferred_element_type=F32)


def mm_t(a, b):
    return lax.dot_general(a, b, (((0,), (0,)), ((), ())), preferred_element_type=F32)


def mm_nt(a, b):
    return lax.dot_general(a, b, (((1,), (1,)), ((), ())), preferred_element_type=F32)


def iota(shape, dim):
    return lax.broadcasted_iota(jnp.int32, shape, dim)


def normalized(x, gain):
    return x * lax.rsqrt(jnp.mean(x * x, -1, keepdims=True) + EPS) * gain


def parts3(x):
    a = x.astype(BF16)
    b = (x - a.astype(F32)).astype(BF16)
    c = (x - a.astype(F32) - b.astype(F32)).astype(BF16)
    return a, b, c


NCH = 8
ROWS = 128
COLS = 512
KVW = 640
FACTOR = 1.4426950408889634 * (NOPE + ROPE) ** -0.5


def moe_kernel(
    rows_ref, gain_ref, idst_ref, wt_ref,
    ql_ref, qgain_ref, kl_ref, kgain_ref, rk_ref, cos_ref, sin_ref, ogain_ref,
    wkv_hbm, sg_hbm, su_hbm, sd_hbm, wq_hbm, wg_hbm, wu_hbm, wd_hbm, wo_hbm,
    mix_ref, out_ref,
    nrm, outq, wkv, sg, su, sd, wq, wg, wu, wd, wo, pick, chi, clo,
    held, part, rly, fin, ret, back, acc,
    kvall, qall, scores, half, other_half,
    w_sem, kv_send, kzr, kzl, kyr, kyl, kyx, q_send, q_recv, half_send, half_recv,
    disp_send, disp_recv, ag_send, agr, agl, agrr, agrl,
    rs_send, rlyr, rlyl, finr, finl, ret_send, ret_recv,
):
    e = lax.axis_index("ep")
    t = lax.axis_index("tp")
    z = e // 8
    k0 = e % 8
    right = (t + 1) % 4
    left = (t + 3) % 4
    opp = (t + 2) % 4
    y = (e // 2) % 4
    core = e % 2
    z_up, z_down = (e + 8) % 64, (e + 56) % 64
    y_up = z * 8 + ((y + 1) % 4) * 2 + core
    y_down = z * 8 + ((y + 3) % 4) * 2 + core
    mate = e + 1 - 2 * core

    barrier = pltpu.get_barrier_semaphore()

    def greet(j, _):
        pl.semaphore_signal(
            barrier, inc=1, device_id={"ep": (e + j) % 64, "tp": t}, device_id_type=MESH
        )
        return 0

    lax.fori_loop(1, 64, greet, 0)
    for other in (right, left):
        pl.semaphore_signal(barrier, inc=1, device_id={"ep": e, "tp": other}, device_id_type=MESH)

    pairs = (
        (wkv_hbm, wkv), (sg_hbm, sg), (su_hbm, su), (sd_hbm, sd), (wq_hbm, wq),
        (wg_hbm, wg), (wu_hbm, wu), (wd_hbm, wd),
    ) + tuple((wo_hbm.at[pl.ds(64 * h, 64)], wo.at[h, pl.ds(64, 64)]) for h in range(4))
    loads = [
        pltpu.make_async_copy(src, dst, w_sem.at[n]) for n, (src, dst) in enumerate(pairs)
    ]
    for load in loads:
        load.start()

    nrm[...] = normalized(rows_ref[...].astype(F32), gain_ref[...]).astype(BF16)

    idst = idst_ref[...]
    member = jnp.zeros((64, ROWS), F32)
    for k in range(4):
        member = member + jnp.where(idst[k : k + 1, :] == iota((64, ROWS), 0), 1.0, 0.0)
    before = jnp.where(iota((ROWS, ROWS), 0) < iota((ROWS, ROWS), 1), 1.0, 0.0).astype(BF16)
    place = (member * (mm(member.astype(BF16), before) + 1.0)).astype(BF16)
    spread = jnp.where((iota((1024, 64), 0) >> 4) == iota((1024, 64), 1), 1.0, 0.0).astype(BF16)
    slot = ((iota((1024, ROWS), 0) & 15) + 1).astype(F32)
    pick[...] = jnp.where(mm(spread, place) == slot, 1.0, 0.0).astype(BF16)
    own_cols = pl.ds(pl.multiple_of(t * COLS, COLS), COLS)
    outq[...] = mm(pick[...], nrm[:, own_cols]).astype(BF16)

    lane = iota((16, ROWS), 1)
    expand = jnp.where(
        jnp.logical_and((lane & 15) == iota((16, ROWS), 0), lane < 32), 1.0, 0.0
    ).astype(BF16)
    cosine = sum(mm_t(p, expand) for p in parts3(cos_ref[...]))
    sine = sum(mm_t(p, expand) for p in parts3(sin_ref[...]))
    sine = jnp.where(iota((ROWS, ROWS), 1) < 16, -sine, sine)

    straight = jnp.where(iota((32, ROWS), 0) == iota((32, ROWS), 1), 1.0, 0.0).astype(BF16)
    swapped = jnp.where(iota((32, ROWS), 0) == (iota((32, ROWS), 1) ^ 16), 1.0, 0.0).astype(BF16)
    rk = rk_ref[...]
    kvall[y, z, :, 512:] = (mm_t(rk, straight) * cosine + mm_t(rk, swapped) * sine).astype(BF16)
    loads[0].wait()
    kvn = normalized(kl_ref[...].astype(F32), kgain_ref[...]).astype(BF16)
    kvall[y, z, :, :512] = mm(kvn, wkv[...]).astype(BF16)

    pl.semaphore_wait(barrier, 65)

    def rows16(k):
        return pl.ds(pl.multiple_of(k * 16, 16), 16)

    def along_ep(src, dst, send_sem, recv_sem, dest):
        return pltpu.make_async_remote_copy(
            src_ref=src, dst_ref=dst, send_sem=send_sem, recv_sem=recv_sem,
            device_id={"ep": dest, "tp": t}, device_id_type=MESH,
        )

    def kv_copy(yi, o, recv_sem, dest):
        block = kvall.at[yi, (z + 8 - o) % 8]
        return along_ep(block, block, kv_send, recv_sem, dest)

    def kv_sideways(o):
        kv_copy(y, o, kyr.at[o], y_up).start()
        kv_copy(y, o, kyl.at[o], y_down).start()

    kv_copy(y, 0, kzr.at[0], z_up).start()
    kv_copy(y, 0, kzl.at[0], z_down).start()
    kv_sideways(0)

    def dispatch(i):
        def one(k, _):
            dest = ((z + 8 - i) % 8) * 8 + k

            @pl.when(dest != e)
            def _():
                along_ep(
                    outq.at[rows16(dest)], held.at[i, t, rows16(k0)], disp_send, disp_recv.at[i], dest
                ).start()

            return 0

        lax.fori_loop(0, 8, one, 0)

    def dispatch_early(i, _):
        dispatch(i)
        return 0

    lax.fori_loop(0, 4, dispatch_early, 0)
    held[0, t, rows16(k0)] = outq[rows16(e)]

    def kv_ring(s):
        kv_copy(y, s + 1, kzr.at[s], z_up).wait_recv()
        if s < 3:
            kv_copy(y, s + 1, kzr.at[s + 1], z_up).start()
        kv_sideways(s + 1)
        if s < 3:
            kv_copy(y, 7 - s, kzl.at[s], z_down).wait_recv()
            if s < 2:
                kv_copy(y, 7 - s, kzl.at[s + 1], z_down).start()
            kv_sideways(7 - s)

    def kv_relay(r):
        for o in {r, (8 - r) % 8}:
            kv_copy((y + 3) % 4, o, kyr.at[o], y_up).wait_recv()
            kv_copy((y + 1) % 4, o, kyl.at[o], y_up).wait_recv()
            if 1 <= o <= 4:
                kv_copy((y + 3) % 4, o, kyx.at[o], y_up).start()
            else:
                kv_copy((y + 1) % 4, o, kyx.at[o], y_down).start()

    def kv_rest():
        for o in range(8):
            kv_copy((y + 2) % 4, o, kyx.at[o], y_up).wait_recv()

    def attend(h):
        cols = pl.ds(pl.multiple_of(h * 128, 128), 128)
        q = jnp.concatenate([qall[0, h], qall[1, h]], axis=0)

        def tile(n):
            yi, zs = n // 2, pl.ds((n % 2) * 4, 4)
            return kvall[yi, zs, :, cols].reshape(512, 128), kvall[yi, zs, :, 512:].reshape(512, 128)

        def first(n, high):
            plain, turned = tile(n)
            s = mm_nt(q, jnp.concatenate([plain, turned], axis=1))
            scores[n] = s
            for b in range(4):
                high = jnp.maximum(high, s[:, b * 128 : (b + 1) * 128])
            return high

        high = lax.fori_loop(0, 8, first, jnp.full((256, 128), -jnp.inf, F32))
        high = jnp.max(high, -1, keepdims=True)

        def second(n, carry):
            total, summed = carry
            p = jnp.exp2((scores[n] - high) * FACTOR)
            for b in range(4):
                total = total + p[:, b * 128 : (b + 1) * 128]
            return total, summed + mm(p.astype(BF16), tile(n)[0])

        zero = jnp.zeros((256, 128), F32)
        total, summed = lax.fori_loop(0, 8, second, (zero, zero))
        total = jnp.sum(total, -1, keepdims=True)
        ln = iota((256, 128), 1)
        summed = jnp.where(ln < 32, high, jnp.where(ln < 64, total, summed))
        half[0, h] = summed[:128]
        half[1, h] = summed[128:]
        along_ep(
            half.at[1 - core, h], other_half.at[h], half_send, half_recv.at[h], mate
        ).start()

    def project():
        head = jnp.zeros((ROWS, 2048), F32)
        ln = iota((ROWS, 128), 1)
        for h in range(4):
            along_ep(
                half.at[1 - core, h], other_half.at[h], half_send, half_recv.at[h], mate
            ).wait_recv()
            one, two = half[core, h], other_half[h]
            top = jnp.maximum(one[:, 0:1], two[:, 0:1])
            w1 = jnp.exp2((one[:, 0:1] - top) * FACTOR)
            w2 = jnp.exp2((two[:, 0:1] - top) * FACTOR)
            value = (one * w1 + two * w2) / (one[:, 32:33] * w1 + two[:, 32:33] * w2)
            value = jnp.where(ln < 64, 0.0, value).astype(BF16)
            head = head + mm(value, wo[h])
        head = head.astype(BF16)
        for q in range(4):
            for b in range(4):
                part[NCH + 1, q, 32 * b : 32 * b + 32] = head[
                    32 * q : 32 * q + 32, COLS * b : COLS * b + COLS
                ]
        scatter_first(NCH + 1)

    def finish_mix():
        mixture = scatter_last(NCH + 1)
        blocks = [mixture[32 * b : 32 * b + 32] for b in range(4)]
        square = sum(jnp.sum(v * v, -1, keepdims=True) for v in blocks) * (1.0 / 2048)
        scale = lax.rsqrt(square + EPS)
        for b in range(4):
            cols = slice(COLS * b, COLS * b + COLS)
            mix_ref[:, cols] = (blocks[b] * scale * ogain_ref[:, cols]).astype(BF16)

    def side(src, dst, send_sem, recv_sem, other):
        return pltpu.make_async_remote_copy(
            src_ref=src, dst_ref=dst, send_sem=send_sem, recv_sem=recv_sem,
            device_id={"ep": e, "tp": other}, device_id_type=MESH,
        )

    lo_half = pl.ds(0, 64)
    hi_half = pl.ds(64, 64)

    def scatter_first(n):
        side(part.at[n, opp, lo_half], rly.at[n, 0], rs_send, rlyr.at[n], right).start()
        side(part.at[n, opp, hi_half], rly.at[n, 1], rs_send, rlyl.at[n], left).start()
        side(part.at[n, right, hi_half], fin.at[n, 0, hi_half], rs_send, finr.at[n], right).start()
        side(part.at[n, left, lo_half], fin.at[n, 1, lo_half], rs_send, finl.at[n], left).start()

    def scatter_second(n):
        side(rly.at[n, 0], rly.at[n, 0], rs_send, rlyr.at[n], right).wait_recv()
        part[n, right, lo_half] = (
            part[n, right, lo_half].astype(F32) + rly[n, 0].astype(F32)
        ).astype(BF16)
        side(part.at[n, right, lo_half], fin.at[n, 0, lo_half], rs_send, finr.at[n], right).start()
        side(rly.at[n, 1], rly.at[n, 1], rs_send, rlyl.at[n], left).wait_recv()
        part[n, left, hi_half] = (
            part[n, left, hi_half].astype(F32) + rly[n, 1].astype(F32)
        ).astype(BF16)
        side(part.at[n, left, hi_half], fin.at[n, 1, hi_half], rs_send, finl.at[n], left).start()

    def scatter_last(n):
        side(fin.at[n, 0], fin.at[n, 0], rs_send, finr.at[n], right).wait_recv()
        side(fin.at[n, 1], fin.at[n, 1], rs_send, finl.at[n], left).wait_recv()
        return part[n, t].astype(F32) + fin[n, 0].astype(F32) + fin[n, 1].astype(F32)

    def swish(g, u):
        return (g / (1.0 + jnp.exp(-g)) * u).astype(BF16)

    for load in loads[1:4]:
        load.wait()
    shared = swish(mm(nrm[...], sg[...]), mm(nrm[...], su[...]))
    for q in range(4):
        part[NCH, q] = mm(shared, sd[:, q * COLS : (q + 1) * COLS]).astype(BF16)
    scatter_first(NCH)
    loads[4].wait()
    qn = normalized(ql_ref[...].astype(F32), qgain_ref[...]).astype(BF16)
    spot = iota((384, 384), 1)
    in_tile = spot & 127
    kind = spot >> 7
    for h in range(4):
        origin = jnp.where(kind == 0, in_tile, 64 + jnp.where(kind == 1, in_tile, in_tile ^ 16))
        valid = in_tile < jnp.where(kind == 0, 64, 32)
        select = jnp.where(
            jnp.logical_and(valid, iota((384, 384), 0) == origin + 96 * h), 1.0, 0.0
        ).astype(BF16)
        three = mm(qn, mm(wq[...], select).astype(BF16))
        qall[core, h, :, :128] = three[:, :128].astype(BF16)
        qall[core, h, :, 128:] = (three[:, 128:256] * cosine + three[:, 256:] * sine).astype(BF16)
    along_ep(qall.at[core], qall.at[core], q_send, q_recv, mate).start()

    wts = wt_ref[...]
    weight = jnp.zeros((64, ROWS), F32)
    for k in range(4):
        weight = weight + jnp.where(
            idst[k : k + 1, :] == iota((64, ROWS), 0), wts[k : k + 1, :], 0.0
        )
    high_part = weight.astype(BF16)
    low_part = (weight - high_part.astype(F32)).astype(BF16)
    chi[...] = (pick[...].astype(F32) * mm(spread, high_part)).astype(BF16)
    clo[...] = (pick[...].astype(F32) * mm(spread, low_part)).astype(BF16)
    wo[:, 0:64] = jnp.zeros((4, 64, 2048), BF16)

    for load in loads[5:]:
        load.wait()

    acc[...] = jnp.zeros_like(acc)

    def arrive(i):
        @pl.when(i == 0)
        def _():
            some = held.at[0, t, pl.ds(0, 112)]
            side(some, some, disp_send, disp_recv.at[0], right).wait_recv()

        @pl.when(i > 0)
        def _():
            whole = held.at[i, t]
            side(whole, whole, disp_send, disp_recv.at[i], right).wait_recv()

        side(held.at[i, t], held.at[i, t], ag_send, agr.at[i], right).start()
        side(held.at[i, t], held.at[i, t], ag_send, agl.at[i], left).start()

    def pass_on(i):
        side(held.at[i, left], held.at[i, left], ag_send, agr.at[i], right).wait_recv()
        side(
            held.at[i, left, lo_half], held.at[i, left, lo_half], ag_send, agrr.at[i], right
        ).start()
        side(held.at[i, right], held.at[i, right], ag_send, agl.at[i], left).wait_recv()
        side(
            held.at[i, right, hi_half], held.at[i, right, hi_half], ag_send, agrl.at[i], left
        ).start()

    def expert(i):
        side(
            held.at[i, opp, lo_half], held.at[i, opp, lo_half], ag_send, agrr.at[i], right
        ).wait_recv()
        side(
            held.at[i, opp, hi_half], held.at[i, opp, hi_half], ag_send, agrl.at[i], left
        ).wait_recv()
        g = jnp.zeros((ROWS, 256), F32)
        u = jnp.zeros((ROWS, 256), F32)
        for q in range(4):
            piece = held[i, q]
            g = g + mm(piece, wg[q * COLS : (q + 1) * COLS, :])
            u = u + mm(piece, wu[q * COLS : (q + 1) * COLS, :])
        hidden = swish(g, u)
        for q in range(4):
            part[i, q] = mm(hidden, wd[:, q * COLS : (q + 1) * COLS]).astype(BF16)
        scatter_first(i)

    def give_back(i):
        ret[i] = scatter_last(i).astype(BF16)

        def one(k, _):
            dest = ((z + i) % 8) * 8 + k

            @pl.when(dest != e)
            def _():
                pltpu.make_async_remote_copy(
                    src_ref=ret.at[i, rows16(k)],
                    dst_ref=back.at[i, rows16(k0)],
                    send_sem=ret_send,
                    recv_sem=ret_recv.at[i],
                    device_id={"ep": dest, "tp": t},
                    device_id_type=MESH,
                ).start()

            return 0

        lax.fori_loop(0, 8, one, 0)

        @pl.when(i == 0)
        def _():
            back[0, rows16(k0)] = ret[0, rows16(k0)]

    def combine(i):
        @pl.when(i == 0)
        def _():
            some = back.at[0, pl.ds(0, 112)]
            side(some, some, ret_send, ret_recv.at[0], right).wait_recv()

        @pl.when(i > 0)
        def _():
            side(back.at[i], back.at[i], ret_send, ret_recv.at[i], right).wait_recv()

        cols = pl.ds(pl.multiple_of(((z + 8 - i) % 8) * 128, 128), 128)
        acc[...] += mm_t(chi[cols, :], back[i]) + mm_t(clo[cols, :], back[i])

    def step(j, _):
        for stage, lag in (
            (arrive, 0), (pass_on, 1), (expert, 2), (scatter_second, 3), (give_back, 4), (combine, 5)
        ):
            @pl.when(jnp.logical_and(j >= lag, j < lag + NCH))
            def _(stage=stage, lag=lag):
                stage(j - lag)

        @pl.when(j == 1)
        def _():
            scatter_second(NCH)

        @pl.when(j == 3)
        def _():
            acc[...] += scatter_last(NCH)

        @pl.when(j < 4)
        def _():
            dispatch(j + 4)

        for s in range(4):
            @pl.when(j == s)
            def _(s=s):
                kv_ring(s)

        for r in range(5):
            @pl.when(j == r)
            def _(r=r):
                kv_relay(r)

        @pl.when(j == 6)
        def _():
            kv_rest()
            along_ep(qall.at[1 - core], qall.at[1 - core], q_send, q_recv, mate).wait_recv()

        @pl.when(jnp.logical_and(j >= 6, j < 10))
        def _():
            attend(j - 6)

        @pl.when(j == 10)
        def _():
            project()

        @pl.when(j == 11)
        def _():
            scatter_second(NCH + 1)

        @pl.when(j == 12)
        def _():
            finish_mix()

        return 0

    lax.fori_loop(0, NCH + 5, step, 0)
    out_ref[...] = acc[...].astype(BF16)

    sent = outq.at[pl.ds(0, 1008)]
    side(sent, sent, disp_send, disp_recv.at[0], right).wait_send()

    def drain(i, _):
        for piece in (held.at[i, 0], held.at[i, 0], held.at[i, 0]):
            side(piece, piece, ag_send, agr.at[0], right).wait_send()
        return 0

    lax.fori_loop(0, NCH, drain, 0)

    def drain_rs(n, _):
        for piece in (part.at[n, 0], part.at[n, 0], part.at[n, 0]):
            side(piece, piece, rs_send, finr.at[0], right).wait_send()
        return 0

    lax.fori_loop(0, NCH + 2, drain_rs, 0)
    for i in range(NCH):
        piece = ret.at[i, pl.ds(0, 112 if i == 0 else 128)]
        side(piece, piece, ret_send, ret_recv.at[0], right).wait_send()

    def drain_kv(n, _):
        kv_copy(y, 0, kzr.at[0], z_up).wait_send()
        return 0

    lax.fori_loop(0, 31, drain_kv, 0)
    along_ep(qall.at[core], qall.at[core], q_send, q_recv, mate).wait_send()
    along_ep(other_half, other_half, half_send, half_recv.at[0], mate).wait_send()


def fused(small, weights):
    vm = pl.BlockSpec(memory_space=pltpu.VMEM)
    anym = pl.BlockSpec(memory_space=pl.ANY)
    dma = pltpu.SemaphoreType.DMA

    def buf(*shape, dtype=BF16):
        return pltpu.VMEM(shape, dtype)

    return pl.pallas_call(
        moe_kernel,
        name="fused",
        out_shape=(
            jax.ShapeDtypeStruct((32, 2048), BF16),
            jax.ShapeDtypeStruct((ROWS, COLS), BF16),
        ),
        in_specs=[vm] * len(small) + [anym] * len(weights),
        out_specs=(vm, vm),
        scratch_shapes=[
            buf(ROWS, 2048), buf(1024, COLS),
            buf(512, 512), buf(2048, 128), buf(2048, 128), buf(128, 2048), buf(768, 384),
            buf(2048, 256), buf(2048, 256), buf(256, 2048), buf(4, 128, 2048),
            buf(1024, ROWS), buf(1024, ROWS), buf(1024, ROWS),
            buf(NCH, 4, ROWS, COLS), buf(NCH + 2, 4, ROWS, COLS), buf(NCH + 2, 2, 64, COLS),
            buf(NCH + 2, 2, ROWS, COLS), buf(NCH, ROWS, COLS), buf(NCH, ROWS, COLS),
            buf(ROWS, COLS, dtype=F32),
            buf(4, 8, ROWS, KVW), buf(2, 4, ROWS, 256), buf(8, 256, 512, dtype=F32),
            buf(2, 4, ROWS, 128, dtype=F32), buf(4, ROWS, 128, dtype=F32),
            dma((12,)), dma, dma((4,)), dma((4,)), dma((8,)), dma((8,)), dma((8,)),
            dma, dma, dma, dma((4,)),
            dma, dma((NCH,)),
            dma, dma((NCH,)), dma((NCH,)), dma((NCH,)), dma((NCH,)),
            dma, dma((NCH + 2,)), dma((NCH + 2,)), dma((NCH + 2,)), dma((NCH + 2,)),
            dma, dma((NCH,)),
        ],
        compiler_params=pltpu.CompilerParams(
            collective_id=0, has_side_effects=True, vmem_limit_bytes=56 * 1024 * 1024
        ),
        cost_estimate=pl.CostEstimate(flops=80_000_000_000, bytes_accessed=8_000_000, transcendentals=0),
    )(*small, *weights)


def per_device(
    query_latent, keyval_latent, rotary_key, query_gain, keyval_gain, query_weight, keyval_weight,
    output_weight, output_gain, second_rows, second_gain, route_ids, route_weights,
    gate_weight, up_weight, down_weight, shared_gate, shared_up, shared_down,
):
    positions = (lax.axis_index("ep") * ROWS).astype(F32) + jnp.arange(ROWS, dtype=F32)
    inverse = 1.0 / ROPE_BASE ** (jnp.arange(ROPE // 2, dtype=F32) * 2.0 / ROPE)
    angles = inverse[:, None] * positions[None, :]
    return fused(
        (
            second_rows, second_gain.reshape(1, -1), route_ids.T, route_weights.T,
            query_latent, query_gain.reshape(1, -1), keyval_latent, keyval_gain.reshape(1, -1),
            rotary_key.T, jnp.cos(angles), jnp.sin(angles), output_gain.reshape(1, -1),
        ),
        (
            keyval_weight, shared_gate, shared_up, shared_down, query_weight,
            gate_weight[0], up_weight[0], down_weight[0], output_weight,
        ),
    )


def solution(mesh):
    placed = (
        P("ep", None), P("ep", None), P("ep", None), P(), P(), P(None, "tp"), P(None, "tp"),
        P("tp", None), P(), P("ep", None), P(), P("ep", None), P("ep", None),
        P("ep", None, "tp"), P("ep", None, "tp"), P("ep", "tp", None),
        P(None, "tp"), P(None, "tp"), P("tp", None),
    )
    return jax.shard_map(
        per_device,
        mesh=mesh,
        in_specs=placed,
        out_specs=(P(("ep", "tp"), None), P("ep", "tp")),
        check_vma=False,
    )
```

time: 274 us -> 136 us (0.50)
  the two profiles are of different devices: /device:TPU:1 before, /device:TPU:24 now
where the time goes in v2:
time: 136 us
  Pallas kernels  131 us (96%)
  local copies, waits for them, and re-layouts  3.52 us (3%)
    pallas_call x1, Pallas kernels, fused(): pl.pallas_call(moe_kernel, name='fused', out_shape=(jax.ShapeDtypeStruct(...  131 us
    unnamed x6, local copies, waits for them, and re-layouts  2.93 us

profile of v2, /device:TPU:24, one launch (start us, length us, event | category | flops | bytes accessed | tf_op | source)
XLA Modules:
  0.0 136.1 jit_solution(6961648848245981878)
XLA Ops:
  0.6 0.0 copy-start.1
  0.7 0.7 copy-done.1
  1.3 0.6 reshape.27.qgain_ref
  1.9 0.7 multiply_sine_fusion
  2.6 131.1 %fused.1 = (bf16[32,2048]{1,0:T(8,128)(2,1)}, bf16[128,512]{1,0:T(8,128)(2,1)}) custom-call(bf16[128,2048]{1,0:T(8,128)(2,1)} %rows_ref.1, f32[1,2048]{1,0:T(1,128)} %bitcast.12, s32[4,128]{1,0:T(4,128)} %bitcast.15, f32[4,128]{1,0:T(4,128)} %bitcast.16, bf16[128,768]{1,0:T(8,128)(2,1)} %ql_ref.1, f32[1,768]{1,0:T(1,128)} %reshape.27.qgain_ref, ...), custom_call_target="tpu_custom_call" | custom-call | flops 80000000000 | bytes 8000000 | tf_op jit(solution)/shard_map/fused/pallas_call | solution.py:515
  133.8 0.0 copy-start
  133.8 1.6 %copy.23 = bf16[32,2048]{1,0:T(8,128)(2,1)} copy(bf16[32,2048]{1,0:T(8,128)(2,1)} %get-tuple-element.6) | data formatting | bytes 262144
  135.4 0.0 copy-done
  135.4 0.7 copy.24
  (2 shorter events, 0.0 us)
Async XLA Ops:
  0.6 0.7 copy-start.1
  133.8 1.6 %copy-start = (bf16[128,512]{1,0:T(8,128)(2,1)S(1)}, bf16[128,512]{1,0:T(8,128)(2,1)}, u32[]{:S(2)}) copy-start(bf16[128,512]{1,0:T(8,128)(2,1)} %get-tuple-element.7) | copy-start | bytes 393220
